TPU v7x, 32 devices: a whole 2x2x4 slice. The times are simulated.
32 devices in a mesh: sp: 8 (over z, y), tp: 4 (over x, core).
Axes of the slice: x: 2, y: 2, z: 4, core: 2. Of those that a mesh axis runs over, the one named last changes fastest.
Arguments:
- tokens: bfloat16 [8192, 2048], P(('sp', 'tp')), may hold values from -6 to 6
- norm_gain: float32 [2048], replicated, may hold values from 0.1 to 1.9
- w_query: bfloat16 [2048, 2048], P(None, 'tp'), may hold values from -0.125 to 0.125
- w_forget: bfloat16 [2048, 2048], P(None, 'tp'), may hold values from -0.125 to 0.125
- w_value: bfloat16 [2048, 2048], P(None, 'tp'), may hold values from -0.125 to 0.125
- w_rgate: bfloat16 [2048, 2048], P(None, 'tp'), may hold values from -0.125 to 0.125
- w_glu_value: bfloat16 [2048, 2048], P(None, 'tp'), may hold values from -0.125 to 0.125
- w_glu_gate: bfloat16 [2048, 2048], P(None, 'tp'), may hold values from -0.125 to 0.125
- forget_gap: float32 [2048], P('tp'), may hold values from 6.1035156e-05 to 0.1
- decay_shift: float32 [8192, 16], P('sp', 'tp'), may hold values from -0.6 to 0, as said below
- head_gain: float32 [128], replicated, may hold values from 0.1 to 1.9
- conv_taps: float32 [31, 2048], P(None, 'tp'), may hold values from -12 to 12
- conv_gain: float32 [2048], P('tp'), may hold values from 0.1 to 1.9
- out_rec: bfloat16 [2048, 2048], P('tp'), may hold values from -0.09375 to 0.09375
- out_conv: bfloat16 [2048, 2048], P('tp'), may hold values from -0.09375 to 0.09375
Outputs:
- mixed: bfloat16 [8192, 2048], P(('sp', 'tp'))
Inputs may be any that keep to these rules, and one draw needn't show every extreme that they name: `decay_shift`: at most zero everywhere.
All inputs are finite; a program needn't handle non-finite values.
Results may differ from a plain program's by a relative error of at most 0.015.
Values may be sent and summed in bfloat16 or wider, within the bound.
A program may use at most 128 MiB of HBM per device.

v0:
```python
import jax
import jax.numpy as jnp
from jax import lax
from jax.sharding import PartitionSpec as P

HEAD = 128
BLOCK = 64


precise_setting = lax.Precision.HIGHEST
norm_epsilon = 1e-05
head_epsilon = 1e-06


def from_behind(value, axis, steps):
    count = lax.axis_size(axis)
    first, last = (max(0, -steps), min(count, count - steps))
    return lax.ppermute(value, axis, [(source, source + steps) for source in range(first, last)])


def layer_norm(values, gain):
    widened = values.astype(jnp.float32)
    row_mean = jnp.mean(widened, axis=-1, keepdims=True)
    centred = widened - row_mean
    row_var = jnp.mean(centred * centred, axis=-1, keepdims=True)
    return centred * lax.rsqrt(row_var + norm_epsilon) * gain


def local_scan(query, key_gate, values, log_forget):
    row_count, head_count, key_width = query.shape
    value_width = values.shape[2]
    block_count = row_count // BLOCK

    def to_blocks(array):
        return array.reshape(block_count, BLOCK, head_count, array.shape[2]).transpose(0, 2, 1, 3)

    def from_blocks(array):
        return array.transpose(0, 2, 1, 3).reshape(row_count, head_count, array.shape[3])

    causal = lax.broadcasted_iota(jnp.int32, (BLOCK, BLOCK), 0) >= lax.broadcasted_iota(
        jnp.int32, (BLOCK, BLOCK), 1
    )

    def advance(carried, inputs):
        current_state, offset = carried
        query_blk, key_block, value_block, log_blk = inputs
        running_total = jnp.cumsum(log_blk, axis=1)
        closing_log = running_total[:, -1:, :]
        query_decayed = query_blk * jnp.exp(running_total)
        scores = jnp.einsum(
            "htk,hsk->hts",
            query_decayed,
            key_block * jnp.exp(-running_total),
            precision=precise_setting,
        )
        scores = jnp.where(causal[None], scores, 0.0)
        output_rows = jnp.einsum("hts,hsv->htv", scores, value_block, precision=precise_setting)
        output_rows = output_rows + jnp.einsum(
            "ori,oiq->orq", query_decayed, current_state, precision=precise_setting
        )
        query_distant = query_blk * jnp.exp(running_total + offset[:, None, :])
        current_state = jnp.exp(closing_log[:, 0, :])[:, :, None] * current_state + jnp.einsum(
            "itp,ito->ipo",
            key_block * jnp.exp(closing_log - running_total),
            value_block,
            precision=precise_setting,
        )
        return ((current_state, offset + closing_log[:, 0, :]), (output_rows, query_distant))

    start_state = jnp.zeros((head_count, key_width, value_width), jnp.float32)
    start_offset = jnp.zeros((head_count, key_width), jnp.float32)
    final, stacked = lax.scan(
        advance,
        (start_state, start_offset),
        (to_blocks(query), to_blocks(key_gate), to_blocks(values), to_blocks(log_forget)),
    )
    return (final[0], final[1], from_blocks(stacked[0]), from_blocks(stacked[1]))


def recur(query_raw, forget_raw, value_raw, rgate_raw, forget_gap, decay_shift, head_gain):
    row_count = query_raw.shape[0]
    head_count = query_raw.shape[1] // HEAD
    query = jax.nn.silu(query_raw.astype(jnp.float32)).reshape(row_count, head_count, HEAD)
    key_gate = forget_gap * jax.nn.sigmoid(-forget_raw.astype(jnp.float32))
    log_forget = jnp.log1p(-key_gate).reshape(row_count, head_count, HEAD) + decay_shift[:, :, None]
    values = value_raw.astype(jnp.float32).reshape(row_count, head_count, HEAD)
    final_state, total_log, nearby_output, query_distant = local_scan(
        query, key_gate.reshape(row_count, head_count, HEAD), values, log_forget
    )
    logs_all = lax.all_gather(total_log[None], "sp", axis=0, tiled=True)
    after_logs = jnp.cumsum(logs_all, axis=0)
    my_index = lax.axis_index("sp")
    own_log = lax.dynamic_index_in_dim(after_logs - logs_all, my_index, 0, keepdims=False)
    segment_piece = lax.all_gather(
        final_state[None].astype(jnp.bfloat16), "sp", axis=0, tiled=True
    ).astype(jnp.float32)
    piece_rows = segment_piece.shape[0]
    indices = jnp.arange(piece_rows, dtype=jnp.int32)
    multiplier = jnp.where(
        (indices < my_index)[:, None, None],
        jnp.exp(jnp.minimum(own_log[None] - after_logs, 0.0)),
        0.0,
    )
    arriving_state = jnp.zeros_like(final_state) + jnp.einsum(
        "dbq,dbqu->bqu", multiplier, segment_piece, precision=precise_setting
    )
    recurrent_branch = nearby_output + jnp.einsum(
        "bji,jiy->bjy", query_distant, arriving_state, precision=precise_setting
    )
    recurrent_branch = (
        recurrent_branch
        * lax.rsqrt(
            jnp.mean(recurrent_branch * recurrent_branch, axis=-1, keepdims=True) + head_epsilon
        )
        * head_gain
    )
    return (
        recurrent_branch.reshape(row_count, head_count * HEAD)
        * jax.nn.silu(rgate_raw.astype(jnp.float32))
    ).astype(jnp.bfloat16)


def convolve(glu_value, glu_gate, conv_taps, conv_gain):
    row_count = glu_value.shape[0]
    mixed_in = (
        glu_value.astype(jnp.float32) * jax.nn.sigmoid(glu_gate.astype(jnp.float32))
    ).astype(jnp.bfloat16)
    reach = conv_taps.shape[0] - 1
    rim = from_behind(mixed_in[row_count - reach :], "sp", 1)
    padded = lax.optimization_barrier(jnp.concatenate([rim, mixed_in], axis=0)).astype(jnp.float32)
    filtered = jnp.zeros(glu_value.shape, jnp.float32)
    for tap_index in range(reach + 1):
        filtered = filtered + conv_taps[tap_index] * padded[tap_index : tap_index + row_count]
    row_sum, row_square = lax.psum(
        (jnp.sum(filtered, axis=1), jnp.sum(filtered * filtered, axis=1)), "tp"
    )
    channels = filtered.shape[1] * lax.axis_size("tp")
    row_mean = row_sum / channels
    row_var = row_square / channels - row_mean * row_mean
    normed = (filtered - row_mean[:, None]) * lax.rsqrt(row_var[:, None] + norm_epsilon) * conv_gain
    return jax.nn.silu(normed).astype(jnp.bfloat16)


def on_device(
    tokens,
    norm_gain,
    w_query,
    w_forget,
    w_value,
    w_rgate,
    w_glu_value,
    w_glu_gate,
    forget_gap,
    decay_shift,
    head_gain,
    conv_taps,
    conv_gain,
    out_rec,
    out_conv,
):
    weights = (w_query, w_forget, w_value, w_rgate, w_glu_value, w_glu_gate)
    normed = layer_norm(lax.all_gather(tokens, "tp", axis=0, tiled=True), norm_gain).astype(
        jnp.bfloat16
    )
    projected_in = jnp.concatenate(
        [
            jnp.dot(normed, weight, preferred_element_type=jnp.float32).astype(jnp.bfloat16)
            for weight in weights
        ],
        axis=1,
    )
    rec_width = w_query.shape[1]
    conv_width = w_glu_value.shape[1]
    query_raw = projected_in[:, 0:rec_width]
    forget_raw = projected_in[:, rec_width : 2 * rec_width]
    value_raw = projected_in[:, 2 * rec_width : 3 * rec_width]
    rgate_raw = projected_in[:, 3 * rec_width : 4 * rec_width]
    glu_value = projected_in[:, 4 * rec_width : 4 * rec_width + conv_width]
    glu_gate = projected_in[:, 4 * rec_width + conv_width : 4 * rec_width + 2 * conv_width]
    conv_out = convolve(glu_value, glu_gate, conv_taps, conv_gain)
    rec_out = recur(query_raw, forget_raw, value_raw, rgate_raw, forget_gap, decay_shift, head_gain)
    return lax.psum_scatter(
        (
            jnp.dot(rec_out, out_rec, preferred_element_type=jnp.float32)
            + jnp.dot(conv_out, out_conv, preferred_element_type=jnp.float32)
        ).astype(jnp.bfloat16),
        "tp",
        scatter_dimension=0,
        tiled=True,
    )


def solution(mesh):
    placed = (
        P(("sp", "tp"), None),
        P(),
        P(None, "tp"),
        P(None, "tp"),
        P(None, "tp"),
        P(None, "tp"),
        P(None, "tp"),
        P(None, "tp"),
        P("tp"),
        P("sp", "tp"),
        P(),
        P(None, "tp"),
        P("tp"),
        P("tp", None),
        P("tp", None),
    )
    return jax.shard_map(
        on_device, mesh=mesh, in_specs=placed, out_specs=P(("sp", "tp"), None), check_vma=False
    )
```

profile of v0, /device:TPU:0, one launch (start us, length us, event | category | flops | bytes accessed | tf_op | source)
XLA Modules:
  0.0 372.3 jit_solution(16107631403860632699)
XLA Ops:
  10.4 35.7 %all-gather.6.cloned.1.call-done = bf16[1024,2048]{1,0:T(8,128)(2,1)} async-done(((bf16[256,2048]{1,0:T(8,128)(2,1)}), bf16[1024,2048]{1,0:T(8,128)(2,1)}) %all-gather.6.cloned.1.call-update) | async-done | bytes 4194320 | tf_op jit(solution)/shard_map/all_gather | solution.py:162
  46.1 3.0 convert_reduce_fusion
  50.8 1.8 fusion.30
  52.7 5.2 %negate_log-plus-one_fusion = (f32[1024,512]{1,0:T(8,128)}, f32[1024,512]{1,0:T(8,128)}) fusion(bf16[1024,2048]{1,0:T(8,128)(2,1)S(1)} %fusion.30, bf16[2048,512]{1,0:T(8,128)(2,1)S(1)} %copy-done.9, f32[512]{0:T(512)S(1)} %copy-done.11), kind=kOutput, calls=%fused_computation.128 | convolution fusion | flops 2150629376 | bytes 10487808 | tf_op jit(solution)/shard_map/dot_general | solution.py:167
  57.9 2.9 reshape.67
  60.8 2.9 reshape_reshape.10
  63.7 3.4 copy.68
  67.1 5.5 %convert_multiply_fusion.1 = f32[1024,512]{1,0:T(8,128)} fusion(bf16[1024,2048]{1,0:T(8,128)(2,1)S(1)} %copy-done.5, bf16[2048,512]{1,0:T(8,128)(2,1)} %param.19), kind=kOutput, calls=%fused_computation.46 | convolution fusion | flops 2150629376 | bytes 8388608 | tf_op jit(solution)/shard_map/dot_general | solution.py:167
  72.6 2.9 reshape_reshape.12
  75.5 6.5 %fusion.70 = f32[1024,512]{1,0:T(8,128)} fusion(bf16[1024,2048]{1,0:T(8,128)(2,1)} %copy-done.4, bf16[2048,512]{1,0:T(8,128)(2,1)} %param.21), kind=kOutput, calls=%fused_computation.136 | convolution fusion | flops 2148532224 | bytes 8388608 | tf_op jit(solution)/shard_map/dot_general | solution.py:167
  82.0 2.9 reshape.71
  84.9 3.2 fusion.68
  88.2 2.6 copy_bitcast_fusion
  90.7 139.9 %while.17 = (s32[]{:T(128)}, f32[4,128,128]{2,1,0:T(8,128)S(1)}, f32[4,128]{1,0:T(4,128)S(1)}, f32[16,4,64,128]{3,2,0,1:T(8,128)}, f32[16,4,64,128]{3,2,0,1:T(8,...) while((s32[]{:T(128)}, f32[4,128,128]{2,1,0:T(8,128)S(1)}, ...), condition=%wide.region_4.0_spmd.clone, body=%wide.region_2.4_spmd.clone.sunk | while | flops 153637888 | bytes 3575959 | solution.py:72
  94.3 1.9 fusion.116
  96.3 1.6 convolution_add_fusion.3
  103.0 1.9 fusion.116
  105.0 1.6 convolution_add_fusion.3
  111.8 1.9 fusion.116
  113.7 1.6 convolution_add_fusion.3
  115.4 1.6 bitcast_dynamic-update-slice_fusion.2
  120.5 1.9 fusion.116
  122.5 1.6 convolution_add_fusion.3
  129.3 1.9 fusion.116
  131.2 1.6 convolution_add_fusion.3
  138.0 1.9 fusion.116
  140.0 1.6 convolution_add_fusion.3
  146.7 1.9 fusion.116
  148.7 1.6 convolution_add_fusion.3
  155.5 1.9 fusion.116
  157.4 1.6 convolution_add_fusion.3
  164.2 1.9 fusion.116
  166.2 1.6 convolution_add_fusion.3
  173.0 1.9 fusion.116
  174.9 1.6 convolution_add_fusion.3
  176.5 1.6 bitcast_dynamic-update-slice_fusion.2
  181.7 1.9 fusion.116
  183.7 1.6 convolution_add_fusion.3
  190.5 1.9 fusion.116
  192.4 1.6 convolution_add_fusion.3
  199.2 1.9 fusion.116
  201.1 1.6 convolution_add_fusion.3
  202.8 1.6 bitcast_dynamic-update-slice_fusion.2
  207.9 1.9 fusion.116
  209.9 1.6 convolution_add_fusion.3
  216.7 1.9 fusion.116
  218.6 1.6 convolution_add_fusion.3
  225.4 1.9 fusion.116
  227.4 1.6 convolution_add_fusion.3
  229.0 1.6 bitcast_dynamic-update-slice_fusion.2
  230.6 2.9 copy.39
  234.3 26.5 %all-gather.2 = f32[8,4,128]{2,1,0:T(4,128)S(1)} all-gather(f32[1,4,128]{2,1,0:T(4,128)S(1)} %bitcast.141), channel_id=2, replica_groups=mesh['sp'=8,'tp'=4] {'sp'}, dimensions={0}, use_global_device_ids=true | all-gather | bytes 18432 | tf_op jit(solution)/shard_map/all_gather | solution.py:90
  260.8 5.3 %convolution_convert_fusion.1 = bf16[1024,512]{1,0:T(8,128)(2,1)S(1)} fusion(bf16[1024,2048]{1,0:T(8,128)(2,1)} %copy-done.4, bf16[2048,512]{1,0:T(8,128)(2,1)} %param.23), kind=kOutput, calls=%fused_computation.132 | convolution fusion | flops 2148007936 | bytes 7340032 | tf_op jit(solution)/shard_map/dot_general | solution.py:167
  266.1 2.6 multiply_convert_fusion.1
  268.8 3.4 collective-permute-start
  274.3 9.5 %fusion.79 = (f32[1024]{0:T(1024)S(1)}, f32[1024]{0:T(1024)S(1)}, f32[1024,512]{1,0:T(8,128)}) fusion(f32[1054,512]{1,0:T(8,128)S(1)} %convert_element_type.79, f32[512]{0:T(512)S(1)} %bitcast.152, f32[512]{0:T(512)S(1)} %bitcast.153, f32[512]{0:T(512)S(1)} %bitcast.155, f32[512]{0:T(512)S(1)} %bitcast.156, f32[512]{0:T(512)S(1)} %bitcast.157, ...), kind=kLoop, calls=%fused_computation.155 | loop fusion | flops 33552384 | bytes 67180544 | tf_op jit(solution)/shard_map/reduce_sum | solution.py:135
  283.8 6.3 %all-reduce = (f32[1024]{0:T(1024)S(1)}, f32[1024]{0:T(1024)S(1)}) all-reduce(f32[1024]{0:T(1024)S(1)} %get-tuple-element.97, f32[1024]{0:T(1024)S(1)} %get-tuple-element.96), channel_id=1, replica_groups=mesh['sp'=8,'tp'=4] {'tp'}, use_global_device_ids=true, to_apply=%region_10.11 | all-reduce | flops 2048 | bytes 16384 | tf_op jit(solution)/shard_map/psum | solution.py:134
  290.2 1.8 multiply_reduce_fusion
  292.0 4.3 %multiply_reduce_fusion.2 = (f32[1024,4]{0,1:T(4,128)S(1)}, f32[1024,4,128]{0,2,1:T(8,128)S(1)}) fusion(f32[1024,4,128]{0,2,1:T(8,128)} %copy.39, f32[4,128,128]{2,1,0:T(8,128)S(1)} %multiply_reduce_fusion, f32[1024,4,128]{2,0,1:T(8,128)} %bitcast.136), kind=kOutput, calls=%fused_computation.127 | convolution fusion | flops 806875136 | bytes 6569984 | tf_op jit(solution)/shard_map/bji,jiy->bjy/dot_general | solution.py:107
  296.3 1.7 multiply_multiply_fusion
  298.1 2.9 copy.50
  301.0 11.4 %fusion.75 = f32[1024,2048]{1,0:T(8,128)} fusion(bf16[512,2048]{1,0:T(8,128)(2,1)S(1)} %copy-done, f32[1024,512]{1,0:T(8,128)} %copy.50, bf16[1024,2048]{1,0:T(8,128)(2,1)} %copy-done.4, bf16[2048,512]{1,0:T(8,128)(2,1)} %param.22), kind=kOutput, calls=%fused_computation.143 | convolution fusion | flops 4299161600 | bytes 18874368 | tf_op jit(solution)/shard_map/dot_general | solution.py:184
  312.3 9.3 %add_convert_fusion = bf16[1024,2048]{1,0:T(8,128)(2,1)} fusion(f32[1024,2048]{1,0:T(8,128)} %fusion.75, bf16[512,2048]{1,0:T(8,128)(2,1)} %param.31, f32[1024,512]{1,0:T(8,128)} %get-tuple-element.120, f32[512]{0:T(512)S(1)} %copy-done.12, f32[1024]{0:T(1024)S(1)} %get-tuple-element.154, f32[1024]{0:T(1024)S(1)} %get-tuple-element.153), kind=kOutput, calls=%fused_computation.43 | convolution fusion | flops 2155872256 | bytes 16787456 | tf_op jit(solution)/shard_map/dot_general | solution.py:185
  321.6 44.1 %reduce-scatter.2.cloned.1.call-done = bf16[256,2048]{1,0:T(8,128)(2,1)} async-done(((bf16[1024,2048]{1,0:T(8,128)(2,1)}), bf16[256,2048]{1,0:T(8,128)(2,1)}) %reduce-scatter.2.cloned.1.call-update) | async-done | bytes 1048592 | tf_op jit(solution)/shard_map/reduce_scatter | solution.py:182
  (179 shorter events, 84.6 us)
Async XLA Ops:
  6.5 294.4 %copy-start = (bf16[512,2048]{1,0:T(8,128)(2,1)S(1)}, bf16[512,2048]{1,0:T(8,128)(2,1)}, u32[]{:S(2)}) copy-start(bf16[512,2048]{1,0:T(8,128)(2,1)} %param.30) | copy-start | bytes 6291460
  6.5 39.6 %all-gather.6.cloned.1.call-start = ((), (), s32[]{:S(2)}) async-start(), calls=%async_computation.1 | async-start | bytes 5242880 | tf_op jit(solution)/shard_map/all_gather | solution.py:162
  7.3 282.9 %all-gather.8.cloned.1.call-start = ((), (), s32[]{:S(2)}) async-start(), calls=%async_computation.3 | async-start | bytes 1179648 | tf_op jit(solution)/shard_map/all_gather | solution.py:94
  46.1 3.4 copy-start.1
  49.6 1.2 copy-start.7
  50.8 1.9 copy-start.9
  50.8 1.9 copy-start.11
  52.7 5.2 %copy-start.4 = (bf16[1024,2048]{1,0:T(8,128)(2,1)}, bf16[1024,2048]{1,0:T(8,128)(2,1)S(1)}, u32[]{:S(2)}) copy-start(bf16[1024,2048]{1,0:T(8,128)(2,1)S(1)} %fusion.30) | copy-start | bytes 12582916
  63.7 3.4 copy-start.5
  84.9 3.2 copy-start.2
  84.9 3.2 copy-start.3
  234.2 131.5 %reduce-scatter.2.cloned.1.call-start = ((), (), s32[]{:S(2)}) async-start(), calls=%async_computation.2 | async-start | bytes 5242880 | tf_op jit(solution)/shard_map/reduce_scatter | solution.py:182
  260.8 5.3 %copy-start.6 = (bf16[1024,2048]{1,0:T(8,128)(2,1)S(1)}, bf16[1024,2048]{1,0:T(8,128)(2,1)}, u32[]{:S(2)}) copy-start(bf16[1024,2048]{1,0:T(8,128)(2,1)} %copy-done.4) | copy-start | bytes 12582916
  260.8 5.4 %copy-start.10 = (bf16[2048,512]{1,0:T(8,128)(2,1)S(1)}, bf16[2048,512]{1,0:T(8,128)(2,1)}, u32[]{:S(2)}) copy-start(bf16[2048,512]{1,0:T(8,128)(2,1)} %param.24) | copy-start | bytes 6291460
  268.8 5.0 %collective-permute-start = (bf16[30,512]{1,0:T(8,128)(2,1)S(1)}, bf16[30,512]{1,0:T(8,128)(2,1)S(1)}, u32[]{:S(2)}, u32[]{:S(2)}) collective-permute-start(bf16[30,512]{1,0:T(8,128)(2,1)S(1)} %slice.257), channel_id=1, source_target_pairs={{0,4},{4,8},{8,12},{12,16},{16,20},{20,24},{24,28},{1,5},{5,9},{9,... | collective-permute-start | bytes 92168 | tf_op jit(solution)/shard_map/ppermute | solution.py:18
  291.9 4.4 %copy-start.8 = (f32[128]{0:T(128)S(1)}, f32[128]{0:T(128)}, u32[]{:S(2)}) copy-start(f32[128]{0:T(128)} %param.27) | copy-start | bytes 1540
  301.0 11.4 %copy-start.12 = (f32[512]{0:T(512)S(1)}, f32[512]{0:T(512)}, u32[]{:S(2)}) copy-start(f32[512]{0:T(512)} %param.29) | copy-start | bytes 6148
Sparse Core Ops, SparseCore 0:
  8.9 37.1 all-gather.5
  234.4 40.2 all-gather.7
  321.7 43.9 reduce-scatter.1
where the time goes:
time: 375 us; the launch traced here: 372 us
  matrix products  147 us (39%)
  waiting for transfers between devices  82.1 us (22%)
  other arithmetic  51.6 us (14%)
  local copies, waits for them, and re-layouts  41.6 us (11%)
  blocking collectives  32.8 us (9%)
  between operations  13.4 us (4%)
    reduce_scatter x1, waiting for transfers between devices, on_device(): lax.psum_scatter((jnp.dot(rec_out, out_rec, preferred_element_type=jnp.fl...  44.1 us
    all_gather x1, waiting for transfers between devices, on_device(): lax.all_gather(tokens, 'tp', axis=0, tiled=True)  35.7 us
    dot_general x16, matrix products, advance(): jnp.einsum('ori,oiq->orq', query_decayed, current_state, precision=precis...  30.8 us
    all_gather x1, blocking collectives, recur(): logs_all = lax.all_gather(total_log[None], 'sp', axis=0, tiled=True)  26.5 us
    dot_general x16, matrix products, advance(): jnp.einsum('itp,ito->ipo', key_block * jnp.exp(closing_log - running_tota...  25.9 us
    dynamic_update_slice x16, other arithmetic, local_scan(): lax.scan(advance, (start_state, start_offset), (to_blocks(query), to_bloc...  25.4 us
    dot_general x5, matrix products, on_device(): jnp.dot(normed, weight, preferred_element_type=jnp.float32)  25.2 us
    dot_general x16, matrix products, advance(): jnp.einsum('htk,hsk->hts', query_decayed, key_block * jnp.exp(-running_to...  21.2 us
  transfers between devices with their start and end apart: 4, of which 3 were waited for; matrix products, arithmetic and copies ran while one was open for 6% of the time, Pallas kernels for 0%

commit v1 on v0

v1 whole, which is shorter than its diff:
```python
import functools

import jax
import jax.numpy as jnp
from jax import lax
from jax.experimental import pallas as pl
from jax.experimental.pallas import tpu as pltpu
from jax.sharding import PartitionSpec as P

CHUNK = 128
PAD = 16

norm_epsilon = 1e-05
head_epsilon = 1e-06


def dot(a, b, dims=((1,), (0,))):
    return lax.dot_general(a, b, (dims, ((), ())), preferred_element_type=jnp.float32)


def from_behind(value, axis, steps):
    count = lax.axis_size(axis)
    first, last = (max(0, -steps), min(count, count - steps))
    return lax.ppermute(value, axis, [(source, source + steps) for source in range(first, last)])


def layer_norm(values, gain):
    widened = values.astype(jnp.float32)
    row_mean = jnp.mean(widened, axis=-1, keepdims=True)
    centred = widened - row_mean
    row_var = jnp.mean(centred * centred, axis=-1, keepdims=True)
    return centred * lax.rsqrt(row_var + norm_epsilon) * gain


def scan_kernel(
    head, q_ref, f_ref, v_ref, gap_ref, shift_ref, near_ref, far_ref, pack_ref, state, offset
):
    step = pl.program_id(0)
    rows, width = q_ref.shape

    @pl.when(step == 0)
    def _():
        state[...] = jnp.zeros_like(state)
        offset[...] = jnp.zeros_like(offset)

    row = lax.broadcasted_iota(jnp.int32, (rows, rows), 0)
    col = lax.broadcasted_iota(jnp.int32, (rows, rows), 1)
    causal = row >= col
    lower = jnp.where(causal, 1.0, 0.0).astype(jnp.bfloat16)
    for h in range(width // head):
        part = slice(h * head, (h + 1) * head)
        query = q_ref[:, part].astype(jnp.float32)
        query = query * jax.nn.sigmoid(query)
        key = gap_ref[:, part] * jax.nn.sigmoid(-f_ref[:, part].astype(jnp.float32))
        log = jnp.log1p(-key) + shift_ref[:, h : h + 1]
        value = v_ref[:, part]
        high = log.astype(jnp.bfloat16)
        low = (log - high.astype(jnp.float32)).astype(jnp.bfloat16)
        total = dot(lower, high) + dot(lower, low)
        closing = total[rows - 1 : rows, :]
        middle = total[rows // 2 - 1 : rows // 2, :]
        query_mid = (query * jnp.exp(total - middle)).astype(jnp.bfloat16)
        key_mid = (key * jnp.exp(middle - total)).astype(jnp.bfloat16)
        scores = jnp.where(causal, dot(query_mid, key_mid, ((1,), (1,))), 0.0)
        query_near = query * jnp.exp(total)
        held = state[h]
        near_ref[:, part] = dot(scores.astype(jnp.bfloat16), value) + dot(
            query_near.astype(jnp.bfloat16), held.astype(jnp.bfloat16), ((1,), (1,))
        )
        far_ref[:, part] = (query_near * jnp.exp(offset[:, part])).astype(jnp.bfloat16)
        key_end = (key * jnp.exp(closing - total)).astype(jnp.bfloat16)
        state[h] = held * jnp.exp(closing) + dot(value, key_end, ((0,), (0,)))
        offset[:, part] = offset[:, part] + closing

    @pl.when(step == pl.num_programs(0) - 1)
    def _():
        place = lax.broadcasted_iota(jnp.int32, (PAD, head), 0)
        for h in range(width // head):
            pack_ref[h, 0:head, :] = state[h].astype(jnp.bfloat16)
            log = offset[:, h * head : (h + 1) * head]
            high = log.astype(jnp.bfloat16).astype(jnp.float32)
            rest = log - high
            mid = rest.astype(jnp.bfloat16).astype(jnp.float32)
            low = rest - mid
            tail = jnp.where(place == 0, high, jnp.where(place == 1, mid, jnp.where(place == 2, low, 0.0)))
            pack_ref[h, head : head + PAD, :] = tail.astype(jnp.bfloat16)


def local_scan(query_raw, forget_raw, value_raw, forget_gap, decay_shift, head):
    rows, width = query_raw.shape
    heads = width // head
    by_row = pl.BlockSpec((CHUNK, width), lambda i: (i, 0))
    whole = lambda shape: pl.BlockSpec(shape, lambda i: (0,) * len(shape))
    return pl.pallas_call(
        functools.partial(scan_kernel, head),
        grid=(rows // CHUNK,),
        in_specs=[
            by_row,
            by_row,
            by_row,
            whole((1, width)),
            pl.BlockSpec((CHUNK, heads), lambda i: (i, 0)),
        ],
        out_specs=[by_row, by_row, whole((heads, head + PAD, head))],
        out_shape=[
            jax.ShapeDtypeStruct((rows, width), jnp.float32),
            jax.ShapeDtypeStruct((rows, width), jnp.bfloat16),
            jax.ShapeDtypeStruct((heads, head + PAD, head), jnp.bfloat16),
        ],
        scratch_shapes=[
            pltpu.VMEM((heads, head, head), jnp.float32),
            pltpu.VMEM((1, width), jnp.float32),
        ],
        compiler_params=pltpu.CompilerParams(dimension_semantics=("arbitrary",)),
        cost_estimate=pl.CostEstimate(
            flops=rows * width * head * 12, bytes_accessed=rows * width * 12, transcendentals=rows * width * 8
        ),
    )(query_raw, forget_raw, value_raw, forget_gap[None], decay_shift)


def arrive(gathered_ref, arriving, head):
    me = lax.axis_index("sp")
    for h in range(arriving.shape[0]):
        arriving_h = jnp.zeros((head, head), jnp.float32)
        for d in range(gathered_ref.shape[0]):
            tail = gathered_ref[d, h, head : head + PAD, :].astype(jnp.float32)
            log = tail[0:1] + tail[1:2] + tail[2:3]
            stepped = arriving_h * jnp.exp(log) + gathered_ref[d, h, 0:head, :].astype(jnp.float32)
            arriving_h = jnp.where(d < me, stepped, arriving_h)
        arriving[h] = arriving_h.astype(jnp.bfloat16)


def finish_rows(head, channels, near, far, rgate, arriving, filtered, row_sum, row_square, conv_gain, head_gain):
    pieces = []
    for h in range(near.shape[1] // head):
        part = slice(h * head, (h + 1) * head)
        rec = near[:, part] + dot(far[:, part], arriving[h], ((1,), (1,)))
        rec = rec * lax.rsqrt(jnp.mean(rec * rec, axis=-1, keepdims=True) + head_epsilon) * head_gain
        gate = rgate[:, part].astype(jnp.float32)
        pieces.append((rec * (gate * jax.nn.sigmoid(gate))).astype(jnp.bfloat16))
    row_mean = row_sum / channels
    row_var = row_square / channels - row_mean * row_mean
    normed = (filtered - row_mean) * lax.rsqrt(row_var + norm_epsilon) * conv_gain
    return jnp.concatenate(pieces, axis=1), (normed * jax.nn.sigmoid(normed)).astype(jnp.bfloat16)


def finish_kernel(
    head, channels, near_ref, far_ref, rgate_ref, gathered_ref, filtered_ref, sum_ref, square_ref,
    conv_gain_ref, head_gain_ref, out_rec_ref, out_conv_ref, out_ref, arriving
):
    @pl.when(pl.program_id(0) == 0)
    def _():
        arrive(gathered_ref, arriving, head)

    rec, conv = finish_rows(
        head, channels, near_ref[...], far_ref[...], rgate_ref[...], arriving, filtered_ref[...],
        sum_ref[...], square_ref[...], conv_gain_ref[...], head_gain_ref[...],
    )
    out_ref[...] = (dot(rec, out_rec_ref[...]) + dot(conv, out_conv_ref[...])).astype(jnp.bfloat16)


def finish(near, far, rgate, gathered, filtered, row_sum, row_square, conv_gain, head_gain, out_rec, out_conv):
    rows, width = near.shape
    heads, head = gathered.shape[1], gathered.shape[3]
    columns = out_rec.shape[1]
    channels = filtered.shape[1] * lax.axis_size("tp")
    tile = min(256, rows)
    by_row = pl.BlockSpec((tile, width), lambda i: (i, 0))
    one = pl.BlockSpec((tile, 1), lambda i: (i, 0))
    whole = lambda shape: pl.BlockSpec(shape, lambda i: (0,) * len(shape))
    return pl.pallas_call(
        functools.partial(finish_kernel, head, channels),
        grid=(rows // tile,),
        in_specs=[
            by_row, by_row, by_row, whole(gathered.shape),
            pl.BlockSpec((tile, filtered.shape[1]), lambda i: (i, 0)), one, one,
            whole((1, filtered.shape[1])), whole((1, head)), whole(out_rec.shape), whole(out_conv.shape),
        ],
        out_specs=pl.BlockSpec((tile, columns), lambda i: (i, 0)),
        out_shape=jax.ShapeDtypeStruct((rows, columns), jnp.bfloat16),
        scratch_shapes=[pltpu.VMEM((heads, head, head), jnp.bfloat16)],
        compiler_params=pltpu.CompilerParams(dimension_semantics=("arbitrary",)),
    )(near, far, rgate, gathered, filtered, row_sum, row_square, conv_gain[None], head_gain[None], out_rec, out_conv)


def convolve(glu_value, glu_gate, conv_taps):
    row_count = glu_value.shape[0]
    mixed_in = (
        glu_value.astype(jnp.float32) * jax.nn.sigmoid(glu_gate.astype(jnp.float32))
    ).astype(jnp.bfloat16)
    reach = conv_taps.shape[0] - 1
    rim = from_behind(mixed_in[row_count - reach :], "sp", 1)
    padded = lax.optimization_barrier(jnp.concatenate([rim, mixed_in], axis=0)).astype(jnp.float32)
    filtered = jnp.zeros(glu_value.shape, jnp.float32)
    for tap_index in range(reach + 1):
        filtered = filtered + conv_taps[tap_index] * padded[tap_index : tap_index + row_count]
    row_sum, row_square = lax.psum(
        (jnp.sum(filtered, axis=1), jnp.sum(filtered * filtered, axis=1)), "tp"
    )
    return filtered, row_sum[:, None], row_square[:, None]


def on_device(
    tokens, norm_gain, w_query, w_forget, w_value, w_rgate, w_glu_value, w_glu_gate, forget_gap,
    decay_shift, head_gain, conv_taps, conv_gain, out_rec, out_conv,
):
    normed = layer_norm(tokens, norm_gain).astype(jnp.bfloat16)
    normed = lax.all_gather(normed, "tp", axis=0, tiled=True)

    def project(weight):
        return jnp.dot(normed, weight, preferred_element_type=jnp.float32).astype(jnp.bfloat16)

    near, far, pack = local_scan(
        project(w_query), project(w_forget), project(w_value), forget_gap, decay_shift, head_gain.shape[0]
    )
    gathered = lax.all_gather(pack[None], "sp", axis=0, tiled=True)
    filtered, row_sum, row_square = convolve(project(w_glu_value), project(w_glu_gate), conv_taps)
    partial = finish(
        near, far, project(w_rgate), gathered, filtered, row_sum, row_square, conv_gain, head_gain, out_rec, out_conv
    )
    return lax.psum_scatter(partial, "tp", scatter_dimension=0, tiled=True)


def solution(mesh):
    placed = (
        P(("sp", "tp"), None),
        P(),
        P(None, "tp"),
        P(None, "tp"),
        P(None, "tp"),
        P(None, "tp"),
        P(None, "tp"),
        P(None, "tp"),
        P("tp"),
        P("sp", "tp"),
        P(),
        P(None, "tp"),
        P("tp"),
        P("tp", None),
        P("tp", None),
    )
    return jax.shard_map(
        on_device, mesh=mesh, in_specs=placed, out_specs=P(("sp", "tp"), None), check_vma=False
    )
```

time: 375 us -> 187 us (0.50)
  matrix products: 147 us -> 23.4 us
  local copies, waits for them, and re-layouts: 41.6 us -> 1.62 us
  other arithmetic: 51.6 us -> 15 us
  Pallas kernels: 0 us -> 22.7 us
  blocking collectives: 32.8 us -> 26.5 us
    dot_general x72 -> x6, matrix products: 147 us -> 23.4 us  [project(): jnp.dot(normed, weight, preferred_element_type=jnp.float32)]
    all_gather x1 -> x0, blocking collectives: 26.5 us -> none  [recur(): logs_all = lax.all_gather(total_log[None], 'sp', axis=0, tiled=True)]
    dynamic_update_slice x16 -> x0, other arithmetic: 25.4 us -> none  [local_scan(): lax.scan(advance, (start_state, start_offset), (to_blocks(query), to_bloc...]
    pallas_call x0 -> x2, Pallas kernels: none -> 22.7 us  [the longest x1 11.9 us: local_scan(): pl.pallas_call(functools.partial(scan_kernel, head), grid=(rows // CHUNK,...]
    psum x1, blocking collectives: 6.32 us -> 26.5 us  [convolve(): lax.psum((jnp.sum(filtered, axis=1), jnp.sum(filtered * filtered, axis=1)...]
    squeeze x16 -> x0, local copies, waits for them, and re-layouts: 14.6 us -> none  [local_scan(): lax.scan(advance, (start_state, start_offset), (to_blocks(query), to_bloc...]
    another operation x3 -> x0, local copies, waits for them, and re-layouts: 9.17 us -> none  [to_blocks(): array.reshape(block_count, BLOCK, head_count, array.shape[2])]
    reshape x3 -> x0, local copies, waits for them, and re-layouts: 8.7 us -> none  [the longest x1 2.92 us: from_blocks(): array.transpose(0, 2, 1, 3).reshape(row_count, head_count, array.shape[3])]
  transfers between devices with their start and end apart: 4 -> 4, of which waited for: 3 -> 2; matrix products, arithmetic and copies ran while one was open for 6% -> 15% of each run, Pallas kernels for 0% -> 6%
where the time goes in v1:
time: 187 us
  waiting for transfers between devices  80.8 us (43%)
  blocking collectives  26.5 us (14%)
  matrix products  23.4 us (13%)
  Pallas kernels  22.7 us (12%)
  other arithmetic  15 us (8%)
  between operations  13.3 us (7%)
  starting transfers between devices  3.78 us (2%)
    reduce_scatter x1, waiting for transfers between devices, on_device(): return lax.psum_scatter(partial, 'tp', scatter_dimension=0, tiled=True)  44.6 us
    all_gather x1, waiting for transfers between devices, on_device(): normed = lax.all_gather(normed, 'tp', axis=0, tiled=True)  36.1 us
    psum x1, blocking collectives, convolve(): lax.psum((jnp.sum(filtered, axis=1), jnp.sum(filtered * filtered, axis=1)...  26.5 us
    dot_general x6, matrix products, project(): jnp.dot(normed, weight, preferred_element_type=jnp.float32)  23.4 us
    pallas_call x1, Pallas kernels, local_scan(): pl.pallas_call(functools.partial(scan_kernel, head), grid=(rows // CHUNK,...  11.9 us
    pallas_call x1, Pallas kernels, finish(): pl.pallas_call(functools.partial(finish_kernel, head, channels), grid=(ro...  10.8 us
    reduce_sum x1, other arithmetic, convolve(): jnp.sum(filtered * filtered, axis=1)  9.82 us
  transfers between devices with their start and end apart: 4, of which 2 were waited for; matrix products, arithmetic and copies ran while one was open for 15% of the time, Pallas kernels for 6%

profile of v1, /device:TPU:0, one launch (start us, length us, event | category | flops | bytes accessed | tf_op | source)
XLA Modules:
  0.0 187.0 jit_solution(17535508714413617580)
XLA Ops:
  6.5 0.0 copy-start
  6.5 0.0 copy-start.1
  6.5 0.0 copy-start.4
  6.5 0.0 all-gather.4.cloned.1.call-start
  6.5 1.6 convert_reduce_fusion
  8.2 0.0 copy-start.3
  8.2 1.6 fusion.2
  9.8 0.0 copy-start.2
  9.8 0.0 copy-done.1
  9.8 0.0 copy-done.4
  9.9 1.4 fusion.4
  11.2 0.0 all-gather.4.cloned.1.call-update
  11.2 0.0 all-gather.6.cloned.1.call-start
  11.3 0.0 copy-done.3
  11.3 1.1 copy.20.shift_ref
  12.4 0.0 copy-done.2
  12.4 36.1 %all-gather.4.cloned.1.call-done = bf16[1024,2048]{1,0:T(8,128)(2,1)} async-done(((bf16[256,2048]{1,0:T(8,128)(2,1)}), bf16[1024,2048]{1,0:T(8,128)(2,1)}) %all-gather.4.cloned.1.call-update) | async-done | bytes 4194320 | tf_op jit(solution)/shard_map/all_gather | solution.py:208
  48.6 0.0 copy-done
  48.6 0.0 copy-start.5
  48.6 0.0 copy-start.6
  48.6 4.7 %convolution_convert_fusion.1 = bf16[1024,512]{1,0:T(8,128)(2,1)S(1)} fusion(bf16[1024,2048]{1,0:T(8,128)(2,1)} %all-gather.4.cloned.1.call-done, bf16[2048,512]{1,0:T(8,128)(2,1)S(1)} %copy-done), kind=kOutput, calls=%fused_computation.71 | convolution fusion | flops 2148007936 | bytes 7340032 | tf_op jit(solution)/shard_map/dot_general | solution.py:211
  53.2 0.0 copy-done.5
  53.2 0.0 copy-done.6
  53.3 0.0 copy-start.7
  53.3 2.6 %multiply_convert_fusion = bf16[1024,512]{1,0:T(8,128)(2,1)S(1)} fusion(bf16[1024,512]{1,0:T(8,128)(2,1)S(1)} %convolution_convert_fusion.1, bf16[1024,2048]{1,0:T(8,128)(2,1)S(1)} %copy-done.5, bf16[2048,512]{1,0:T(8,128)(2,1)S(1)} %copy-done.6), kind=kOutput, calls=%fused_computation.69 | convolution fusion | flops 2151677952 | bytes 8388608 | tf_op jit(solution)/shard_map/dot_general | solution.py:211
  55.9 0.0 copy-start.8
  55.9 3.5 %collective-permute-start = (bf16[30,512]{1,0:T(8,128)(2,1)S(1)}, bf16[30,512]{1,0:T(8,128)(2,1)S(1)}, u32[]{:S(2)}, u32[]{:S(2)}) collective-permute-start(bf16[30,512]{1,0:T(8,128)(2,1)S(1)} %slice.252), channel_id=1, source_target_pairs={{0,4},{4,8},{8,12},{12,16},{16,20},{20,24},{24,28},{1,5},{5,9},{9,... | collective-permute-start | bytes 92168 | tf_op jit(solution)/shard_map/ppermute | solution.py:24
  59.4 0.0 copy-done.7
  59.5 3.3 %convolution_convert_fusion.3.v_ref = bf16[1024,512]{1,0:T(8,128)(2,1)} fusion(bf16[1024,2048]{1,0:T(8,128)(2,1)S(1)} %copy-done.5, bf16[2048,512]{1,0:T(8,128)(2,1)S(1)} %copy-done.7), kind=kOutput, calls=%fused_computation.73 | convolution fusion | flops 2148007936 | bytes 7340032 | tf_op jit(solution)/shard_map/dot_general | solution.py:211
  62.8 0.0 copy-done.8
  62.8 0.0 copy-start.9
  62.8 3.3 %convolution_convert_fusion.4.f_ref = bf16[1024,512]{1,0:T(8,128)(2,1)} fusion(bf16[1024,2048]{1,0:T(8,128)(2,1)S(1)} %copy-done.5, bf16[2048,512]{1,0:T(8,128)(2,1)S(1)} %copy-done.8), kind=kOutput, calls=%fused_computation.74 | convolution fusion | flops 2148007936 | bytes 7340032 | tf_op jit(solution)/shard_map/dot_general | solution.py:211
  66.1 0.0 copy-done.9
  66.1 3.3 %convolution_convert_fusion.5.q_ref = bf16[1024,512]{1,0:T(8,128)(2,1)} fusion(bf16[1024,2048]{1,0:T(8,128)(2,1)S(1)} %copy-done.5, bf16[2048,512]{1,0:T(8,128)(2,1)S(1)} %copy-done.9), kind=kOutput, calls=%fused_computation.75 | convolution fusion | flops 2148007936 | bytes 7340032 | tf_op jit(solution)/shard_map/dot_general | solution.py:211
  69.4 11.9 %shard_map.145 = (f32[1024,512]{1,0:T(8,128)}, bf16[1024,512]{1,0:T(8,128)(2,1)}, bf16[4,144,128]{2,1,0:T(8,128)(2,1)}) custom-call(bf16[1024,512]{1,0:T(8,128)(2,1)} %convolution_convert_fusion.5.q_ref, bf16[1024,512]{1,0:T(8,128)(2,1)} %convolution_convert_fusion.4.f_ref, bf16[1024,512]{1,0:T(8,128)(2,1)} %convolution_convert_fusion.3.v_ref, ...), custom_call_target="tpu_custom_call" | custom-call | flops 805306368 | bytes 6291456 | tf_op jit(solution)/shard_map/pallas_call | solution.py:94
  81.3 0.0 all-gather.6.cloned.1.call-update
  81.4 0.2 reduce-scatter.2.cloned.1.call-start
  81.6 6.2 %convolution_convert_fusion.2.rgate_ref = bf16[1024,512]{1,0:T(8,128)(2,1)} fusion(bf16[1024,2048]{1,0:T(8,128)(2,1)} %all-gather.4.cloned.1.call-done, bf16[2048,512]{1,0:T(8,128)(2,1)} %param.20), kind=kOutput, calls=%fused_computation.72 | convolution fusion | flops 2148007936 | bytes 7340032 | tf_op jit(solution)/shard_map/dot_general | solution.py:211
  87.8 0.0 collective-permute-done
  87.8 0.3 pad_maximum_fusion
  88.0 0.3 convert_element_type.47
  88.3 9.8 %multiply_reduce_fusion = (f32[1024]{0:T(1024)S(1)}, f32[1024]{0:T(1024)S(1)}, f32[1024,512]{1,0:T(8,128)}) fusion(f32[1054,512]{1,0:T(8,128)S(1)} %convert_element_type.47, f32[512]{0:T(512)S(1)} %bitcast.62, f32[512]{0:T(512)S(1)} %bitcast.63, f32[512]{0:T(512)S(1)} %bitcast.65, f32[512]{0:T(512)S(1)} %bitcast.66, f32[512]{0:T(512)S(1)} %bitcast.67, ...), kind=kLoop, calls=%fused_computation.68 | loop fusion | flops 33552384 | bytes 67180544 | tf_op jit(solution)/shard_map/reduce_sum | solution.py:198
  98.1 0.2 copy.21
  98.4 0.2 copy.22
  98.6 26.5 %all-reduce = (f32[1024,1]{1,0:T(8,128)}, f32[1024,1]{1,0:T(8,128)}) all-reduce(f32[1024,1]{1,0:T(8,128)S(1)} %copy.21, f32[1024,1]{1,0:T(8,128)S(1)} %copy.22), channel_id=1, replica_groups=mesh['sp'=8,'tp'=4] {'tp'}, use_global_device_ids=true, to_apply=%region_3.0 | all-reduce | flops 2048 | bytes 16384 | tf_op jit(solution)/shard_map/psum | solution.py:197
  125.1 0.0 all-gather.6.cloned.1.call-done
  125.1 10.8 %shard_map.146 = bf16[1024,2048]{1,0:T(8,128)(2,1)} custom-call(f32[1024,512]{1,0:T(8,128)} %get-tuple-element.8.near_ref, bf16[1024,512]{1,0:T(8,128)(2,1)} %get-tuple-element.9.far_ref, bf16[1024,512]{1,0:T(8,128)(2,1)} %convolution_convert_fusion.2.rgate_ref, bf16[8,4,144,128]{3,2,1,0:T(8,128)(2,1)} %bitcast.49, ...), custom_call_target="tpu_custom_call" | custom-call | tf_op jit(solution)/shard_map/pallas_call | solution.py:171
  135.9 0.0 reduce-scatter.2.cloned.1.call-update
  135.9 44.6 %reduce-scatter.2.cloned.1.call-done = bf16[256,2048]{1,0:T(8,128)(2,1)} async-done(((bf16[1024,2048]{1,0:T(8,128)(2,1)}), bf16[256,2048]{1,0:T(8,128)(2,1)}) %reduce-scatter.2.cloned.1.call-update) | async-done | bytes 1048592 | tf_op jit(solution)/shard_map/reduce_scatter | solution.py:221
  (5 shorter events, 0.1 us)
Async XLA Ops:
  6.5 42.0 %copy-start = (bf16[2048,512]{1,0:T(8,128)(2,1)S(1)}, bf16[2048,512]{1,0:T(8,128)(2,1)}, u32[]{:S(2)}) copy-start(bf16[2048,512]{1,0:T(8,128)(2,1)} %param.21) | copy-start | bytes 6291460
  6.5 3.3 %copy-start.1 = (bf16[256,2048]{1,0:T(8,128)(2,1)S(1)}, bf16[256,2048]{1,0:T(8,128)(2,1)}, u32[]{:S(2)}) copy-start(bf16[256,2048]{1,0:T(8,128)(2,1)} %param.15) | copy-start | bytes 3145732
  6.5 3.3 %copy-start.4 = (f32[2048]{0:T(1024)S(1)}, f32[2048]{0:T(1024)}, u32[]{:S(2)}) copy-start(f32[2048]{0:T(1024)} %param.16) | copy-start | bytes 24580
  6.5 42.0 %all-gather.4.cloned.1.call-start = ((), (), s32[]{:S(2)}) async-start(), calls=%async_computation.1 | async-start | bytes 5242880 | tf_op jit(solution)/shard_map/all_gather | solution.py:208
  8.2 3.1 %copy-start.3 = (f32[1024,4]{0,1:T(4,128)S(1)}, f32[1024,4]{0,1:T(4,128)}, u32[]{:S(2)}) copy-start(f32[1024,4]{0,1:T(4,128)} %param.24) | copy-start | bytes 49156
  9.8 2.6 %copy-start.2 = (f32[31,512]{1,0:T(8,128)S(1)}, f32[31,512]{1,0:T(8,128)}, u32[]{:S(2)}) copy-start(f32[31,512]{1,0:T(8,128)} %param.26) | copy-start | bytes 190468
  11.2 113.9 %all-gather.6.cloned.1.call-start = ((), (), s32[]{:S(2)}) async-start(), calls=%async_computation.3 | async-start | bytes 1327104 | tf_op jit(solution)/shard_map/all_gather | solution.py:216
  48.6 4.7 %copy-start.5 = (bf16[1024,2048]{1,0:T(8,128)(2,1)S(1)}, bf16[1024,2048]{1,0:T(8,128)(2,1)}, u32[]{:S(2)}) copy-start(bf16[1024,2048]{1,0:T(8,128)(2,1)} %all-gather.4.cloned.1.call-done) | copy-start | bytes 12582916
  48.6 4.7 %copy-start.6 = (bf16[2048,512]{1,0:T(8,128)(2,1)S(1)}, bf16[2048,512]{1,0:T(8,128)(2,1)}, u32[]{:S(2)}) copy-start(bf16[2048,512]{1,0:T(8,128)(2,1)} %param.22) | copy-start | bytes 6291460
  53.3 6.2 %copy-start.7 = (bf16[2048,512]{1,0:T(8,128)(2,1)S(1)}, bf16[2048,512]{1,0:T(8,128)(2,1)}, u32[]{:S(2)}) copy-start(bf16[2048,512]{1,0:T(8,128)(2,1)} %param.19) | copy-start | bytes 6291460
  55.9 6.9 %copy-start.8 = (bf16[2048,512]{1,0:T(8,128)(2,1)S(1)}, bf16[2048,512]{1,0:T(8,128)(2,1)}, u32[]{:S(2)}) copy-start(bf16[2048,512]{1,0:T(8,128)(2,1)} %param.18) | copy-start | bytes 6291460
  55.9 31.8 %collective-permute-start = (bf16[30,512]{1,0:T(8,128)(2,1)S(1)}, bf16[30,512]{1,0:T(8,128)(2,1)S(1)}, u32[]{:S(2)}, u32[]{:S(2)}) collective-permute-start(bf16[30,512]{1,0:T(8,128)(2,1)S(1)} %slice.252), channel_id=1, source_target_pairs={{0,4},{4,8},{8,12},{12,16},{16,20},{20,24},{24,28},{1,5},{5,9},{9,... | collective-permute-start | bytes 92168 | tf_op jit(solution)/shard_map/ppermute | solution.py:24
  62.8 3.3 %copy-start.9 = (bf16[2048,512]{1,0:T(8,128)(2,1)S(1)}, bf16[2048,512]{1,0:T(8,128)(2,1)}, u32[]{:S(2)}) copy-start(bf16[2048,512]{1,0:T(8,128)(2,1)} %param.17) | copy-start | bytes 6291460
  81.4 99.1 %reduce-scatter.2.cloned.1.call-start = ((), (), s32[]{:S(2)}) async-start(), calls=%async_computation.2 | async-start | bytes 5242880 | tf_op jit(solution)/shard_map/reduce_scatter | solution.py:221
Sparse Core Ops, SparseCore 0:
  11.4 37.1 all-gather.3
  81.5 40.1 all-gather.5
  136.1 44.3 reduce-scatter.1
